TPU v7x, 32 devices: a whole 2x2x4 slice. The times are simulated.
32 devices in a mesh: fs: 8 (over z, x), tp: 4 (over y, core).
Axes of the slice: x: 2, y: 2, z: 4, core: 2. Of those that a mesh axis runs over, the one named last changes fastest.
Arguments:
- inputs: bfloat16 [3072, 2048], P('fs'), may hold values from -6 to 6
- queries: bfloat16 [3072, 2048], P('fs', 'tp'), may hold values from -6 to 6
- keys: bfloat16 [3072, 2048], P('fs', 'tp'), may hold values from -6 to 6
- values: bfloat16 [3072, 2048], P('fs', 'tp'), may hold values from -6 to 6
- head_cot: bfloat16 [3072, 2048], P('fs', 'tp'), may hold values from -6 to 6
- mixing: float32 [16], P('tp'), may hold values from 0.3 to 0.8
- head_gain: float32 [128], replicated, may hold values from 0.1 to 1.9
- factors: bfloat16 [2048, 2, 256], P('fs'), may hold values from -0.375 to 0.375
- moments: float32 [256, 2, 2048], P('fs', None, 'tp'), may hold values from -6 to 6
- weights: float32 [2048, 2, 2048], P('fs', None, 'tp'), may hold values from -6 to 6
Outputs:
- step: float32 [2048, 2, 2048], P('fs', None, 'tp')
- new_moments: float32 [256, 2, 2048], P('fs', None, 'tp')
- copies: bfloat16 [2048, 2, 2048], P(None, None, 'tp')
All inputs are finite; a program needn't handle non-finite values.
Results may differ from a plain program's by a relative error of at most 0.007.
Values may be sent and summed in bfloat16 or wider, within the bound.
A program may use at most 64 MiB of HBM per device.

v0:
```python
import jax
import jax.numpy as jnp
from jax import lax
from jax.sharding import PartitionSpec as P

EPS = 0.05
BETA = 0.9
RATE_BASE = 0.5


def softmax_rows(scores):
    top = jnp.max(scores, axis=-1, keepdims=True)
    expo = jnp.exp(scores - top)
    return expo / jnp.sum(expo, axis=-1, keepdims=True)


def head_grads(query, key_rows, value, upstream, weight_mix, head_gain):
    length = query.shape[0]
    head_dim = query.shape[2]
    factor = head_dim ** (-0.5)
    places = jnp.arange(length)
    causal = places[None, :] <= places[:, None]

    def probs(which):
        scores = (
            jnp.dot(query[:, which], key_rows[:, which].T, preferred_element_type=jnp.float32)
            * factor
        )
        return softmax_rows(jnp.where(causal, scores, -jnp.inf))

    first = probs(0)
    second = probs(1)
    mixed = (first - weight_mix * second).astype(jnp.bfloat16)
    output = jnp.dot(mixed, value, preferred_element_type=jnp.float32)
    inverse = lax.rsqrt(jnp.mean(output * output, axis=-1, keepdims=True) + EPS)
    scaled = head_gain * upstream.astype(jnp.float32)
    d_out = inverse * scaled - output * inverse**3 * jnp.mean(
        output * scaled, axis=-1, keepdims=True
    )
    d_out = d_out.astype(jnp.bfloat16)
    d_value = jnp.dot(mixed.T, d_out, preferred_element_type=jnp.float32).astype(jnp.bfloat16)
    d_mix = jnp.dot(d_out, value.T, preferred_element_type=jnp.float32)
    d_first = (first * (d_mix - jnp.sum(first * d_mix, axis=-1, keepdims=True))).astype(
        jnp.bfloat16
    )
    d_second = (
        -weight_mix * second * (d_mix - jnp.sum(second * d_mix, axis=-1, keepdims=True))
    ).astype(jnp.bfloat16)
    q_first = (
        jnp.dot(d_first, key_rows[:, 0], preferred_element_type=jnp.float32) * factor
    ).astype(jnp.bfloat16)
    q_second = (
        jnp.dot(d_second, key_rows[:, 1], preferred_element_type=jnp.float32) * factor
    ).astype(jnp.bfloat16)
    return (jnp.stack([q_first, q_second], axis=1).reshape(length, 2 * head_dim), d_value)


def per_device(
    inputs, queries, keys, values, head_cot, mixing, head_gain, factors, moments, weights
):
    length = inputs.shape[0]
    heads_here = mixing.shape[0]
    head_width = values.shape[1] // heads_here
    head_dim = head_width // 2
    query_heads = queries.reshape(length, heads_here, 2, head_dim).transpose(1, 0, 2, 3)
    key_heads = keys.reshape(length, heads_here, 2, head_dim).transpose(1, 0, 2, 3)
    value_heads = values.reshape(length, heads_here, head_width).transpose(1, 0, 2)
    upstream_heads = head_cot.reshape(length, heads_here, head_width).transpose(1, 0, 2)

    def one_head(pieces):
        return head_grads(pieces[0], pieces[1], pieces[2], pieces[3], pieces[4], head_gain)

    d_query, d_value = lax.map(
        one_head, (query_heads, key_heads, value_heads, upstream_heads, mixing)
    )
    d_query = d_query.transpose(1, 0, 2).reshape(length, heads_here * head_width)
    d_value = d_value.transpose(1, 0, 2).reshape(length, heads_here * head_width)
    cotangents = jnp.stack([d_query, d_value], axis=1)
    fs_count = lax.axis_size("fs")
    token_factor = (length * fs_count) ** (-0.5)
    rank_here = moments.shape[0]
    cols_here = moments.shape[2]
    factor_wide = factors.astype(jnp.float32)
    whole_factors = lax.all_gather(factors, "fs", axis=0, tiled=True)
    reduced = jnp.einsum("td,dkr->tkr", inputs, whole_factors, preferred_element_type=jnp.float32)
    reduced_upper = reduced.astype(jnp.bfloat16)
    reduced_lower = (reduced - reduced_upper.astype(jnp.float32)).astype(jnp.bfloat16)
    upper_part = jnp.einsum(
        "tkr,tke->rke", reduced_upper, cotangents, preferred_element_type=jnp.float32
    )
    lower_part = jnp.einsum(
        "tkr,tke->rke", reduced_lower, cotangents, preferred_element_type=jnp.float32
    )
    projected = lax.psum_scatter(upper_part + lower_part, "fs", scatter_dimension=0, tiled=True)
    projected = projected * token_factor
    new_moments = BETA * moments + projected
    local_sums = jnp.sum(new_moments * new_moments, axis=(0, 2))
    totals = lax.psum(local_sums, ("fs", "tp"))
    entries = rank_here * fs_count * cols_here * lax.axis_size("tp")
    rate = RATE_BASE / jnp.sqrt(1.0 + totals / entries)
    low_part = jnp.einsum(
        "dkr,rke->dke",
        factor_wide,
        lax.all_gather(new_moments, "fs", axis=0, tiled=True),
        precision=lax.Precision.HIGHEST,
    )
    step = low_part * rate[None, :, None]
    copies = lax.all_gather((weights - step).astype(jnp.bfloat16), "fs", axis=0, tiled=True)
    return (step, new_moments, copies)


def solution(mesh):
    placed = (
        P("fs", None),
        P("fs", "tp"),
        P("fs", "tp"),
        P("fs", "tp"),
        P("fs", "tp"),
        P("tp"),
        P(),
        P("fs", None, None),
        P("fs", None, "tp"),
        P("fs", None, "tp"),
    )
    return jax.shard_map(
        per_device,
        mesh=mesh,
        in_specs=placed,
        out_specs=(P("fs", None, "tp"), P("fs", None, "tp"), P(None, None, "tp")),
        check_vma=False,
    )
```

profile of v0, /device:TPU:0, one launch (start us, length us, event | category | flops | bytes accessed | tf_op | source)
XLA Modules:
  0.0 282.7 jit_solution(10454785109164463003)
XLA Ops:
  7.3 1.8 copy.46
  9.2 1.2 copy.39
  10.4 1.2 copy.40
  11.8 1.2 copy.42
  13.0 21.3 %while.12 = (s32[]{:T(128)}, bf16[4,384,128]{1,2,0:T(8,128)(2,1)S(1)}, bf16[4,384,128]{2,1,0:T(8,128)(2,1)}, bf16[4,384,2,64]{1,3,2,0:T(8,128)(2,1)S(1)}, bf16[4...) while((s32[]{:T(128)}, ...), condition=%wide.region_9.10_spmd, body=%wide.region_0.9_spmd.sunk | while | flops 195525504 | bytes 10978449 | solution.py:73
  13.1 0.6 dynamic_slice.47
  14.3 0.3 fusion.67
  14.8 0.3 fusion.65
  15.2 0.8 subtract_convert_fusion.5
  16.3 1.0 fusion.71
  17.3 0.4 multiply_reduce_fusion.7
  18.0 0.3 fusion.69
  18.4 0.6 dynamic_slice.47
  19.6 0.3 fusion.67
  20.1 0.3 fusion.65
  20.5 0.8 subtract_convert_fusion.5
  21.6 1.0 fusion.71
  22.6 0.4 multiply_reduce_fusion.7
  23.3 0.3 fusion.69
  23.7 0.6 dynamic_slice.47
  25.0 0.3 fusion.67
  25.4 0.3 fusion.65
  25.8 0.8 subtract_convert_fusion.5
  26.9 1.0 fusion.71
  27.9 0.4 multiply_reduce_fusion.7
  28.7 0.3 fusion.69
  29.0 0.6 dynamic_slice.47
  30.3 0.3 fusion.67
  30.7 0.3 fusion.65
  31.2 0.8 subtract_convert_fusion.5
  32.3 1.0 fusion.71
  33.3 0.4 multiply_reduce_fusion.7
  34.0 0.3 fusion.69
  34.3 1.2 copy.45
  35.6 27.0 %all-gather.4.cloned.1.call-done = bf16[2048,2,256]{2,0,1:T(8,128)(2,1)} async-done(((bf16[256,2,256]{2,0,1:T(8,128)(2,1)}), bf16[2048,2,256]{2,0,1:T(8,128)(2,1)}) %all-gather.4.cloned.1.call-update) | async-done | bytes 2097168 | tf_op jit(solution)/shard_map/all_gather | solution.py:84
  62.6 2.6 fusion.30
  65.2 0.4 fusion.35
  65.6 0.4 fusion.32
  66.1 1.3 copy.47
  67.5 0.6 dynamic-slice
  68.7 75.5 %all-reduce.3.cloned.1.call-done = f32[256,2,512]{2,1,0:T(2,128)} async-done(((f32[256,2,512]{2,1,0:T(2,128)}), f32[256,2,512]{2,1,0:T(2,128)}) %all-reduce.3.cloned.1.call-update) | async-done | bytes 1048592
  144.3 1.8 multiply_reduce_fusion.3
  146.1 1.4 copy.50
  147.6 39.7 %psum.7 = f32[2]{0:T(128)S(1)} all-reduce(f32[2]{0:T(128)S(1)} %get-tuple-element.111), channel_id=1, replica_groups=mesh['fs'=8,'tp'=4] {'fs','tp'}, use_global_device_ids=true, to_apply=%region_12.13 | all-reduce | flops 2 | bytes 16 | tf_op jit(solution)/shard_map/psum | solution.py:98
  187.3 3.5 %subtract_convert_fusion.1 = (bf16[256,2,512]{0,2,1:T(8,128)(2,1)}, f32[256,2,512]{0,2,1:T(8,128)S(1)}) fusion(f32[256,2,512]{0,2,1:T(8,128)} %copy.50, f32[2]{0:T(128)S(1)} %rsqrt_multiply_fusion, bf16[256,2,256]{2,1,0:T(2,128)(2,1)S(1)} %copy-done.1, f32[256,2,512]{2,1,0:T(2,128)} %all-gather.6.cloned.1.call-done), kind=kOutput, calls=%fused_computation.61 | convolution fusion | flops 806092800 | bytes 3932168 | tf_op jit(solution)/shard_map/dkr,rke->dke/dot_general | solution.py:101
  190.8 1.3 copy.51
  192.1 72.9 %all-gather.8.cloned.1.call-done = bf16[2048,2,512]{0,2,1:T(8,128)(2,1)} async-done(((bf16[256,2,512]{0,2,1:T(8,128)(2,1)}), bf16[2048,2,512]{0,2,1:T(8,128)(2,1)}) %all-gather.8.cloned.1.call-update) | async-done | bytes 4194320 | tf_op jit(solution)/shard_map/all_gather | solution.py:108
  265.0 11.1 %copy.52 = bf16[2048,2,512]{2,1,0:T(2,128)(2,1)} copy(bf16[2048,2,512]{0,2,1:T(8,128)(2,1)} %all-gather.8.cloned.1.call-done) | data formatting | bytes 8388608
  (65 shorter events, 3.9 us)
Async XLA Ops:
  7.2 55.4 %copy-start = (bf16[384,2048]{1,0:T(8,128)(2,1)S(1)}, bf16[384,2048]{1,0:T(8,128)(2,1)}, u32[]{:S(2)}) copy-start(bf16[384,2048]{1,0:T(8,128)(2,1)} %param.12) | copy-start | bytes 4718596
  7.2 4.4 %copy-start.3 = (bf16[384,512]{1,0:T(8,128)(2,1)S(1)}, bf16[384,512]{1,0:T(8,128)(2,1)}, u32[]{:S(2)}) copy-start(bf16[384,512]{1,0:T(8,128)(2,1)} %param.15) | copy-start | bytes 1179652
  7.2 5.8 %copy-start.5 = (f32[128]{0:T(128)S(1)}, f32[128]{0:T(128)}, u32[]{:S(2)}) copy-start(f32[128]{0:T(128)} %param.18) | copy-start | bytes 1540
  7.2 5.8 %copy-start.6 = (f32[4]{0:T(128)S(1)}, f32[4]{0:T(128)}, u32[]{:S(2)}) copy-start(f32[4]{0:T(128)} %param.17) | copy-start | bytes 52
  7.2 55.4 %all-gather.4.cloned.1.call-start = ((), (), s32[]{:S(2)}) async-start(), calls=%async_computation | async-start | bytes 2359296 | tf_op jit(solution)/shard_map/all_gather | solution.py:84
  9.1 135.2 %all-reduce.3.cloned.1.call-start = ((), (), s32[]{:S(2)}) async-start(), calls=%async_computation.3 | async-start | bytes 2097152
  66.1 1.4 copy-start.7
  66.1 78.2 %copy-start.4 = (f32[32,2,512]{2,1,0:T(2,128)S(1)}, f32[32,2,512]{2,1,0:T(2,128)}, u32[]{:S(2)}) copy-start(f32[32,2,512]{2,1,0:T(2,128)} %param.20) | copy-start | bytes 393220
  67.4 78.8 %copy-start.2 = (f32[256,2,512]{2,1,0:T(2,128)S(1)}, f32[256,2,512]{2,1,0:T(2,128)}, u32[]{:S(2)}) copy-start(f32[256,2,512]{2,1,0:T(2,128)} %param.21) | copy-start | bytes 3145732
  67.4 119.9 %copy-start.1 = (bf16[256,2,256]{2,1,0:T(2,128)(2,1)S(1)}, bf16[256,2,256]{2,1,0:T(2,128)(2,1)}, u32[]{:S(2)}) copy-start(bf16[256,2,256]{2,1,0:T(2,128)(2,1)} %param.19) | copy-start | bytes 786436
  67.4 119.9 %all-gather.6.cloned.1.call-start = ((), (), s32[]{:S(2)}) async-start(), calls=%async_computation.1 | async-start | bytes 1179648 | tf_op jit(solution)/shard_map/all_gather | solution.py:104
  146.1 118.9 %all-gather.8.cloned.1.call-start = ((), (), s32[]{:S(2)}) async-start(), calls=%async_computation.2 | async-start | bytes 4718592 | tf_op jit(solution)/shard_map/all_gather | solution.py:108
Sparse Core Ops, SparseCore 0:
  10.8 51.7 all-gather.3
  67.5 76.6 all-reduce.2
  147.0 40.0 all-gather.5
  190.9 74.0 all-gather.7
where the time goes:
time: 283 us
  waiting for transfers between devices  176 us (62%)
  blocking collectives  39.7 us (14%)
  local copies, waits for them, and re-layouts  25.2 us (9%)
  matrix products  18.3 us (6%)
  between operations  14.6 us (5%)
  other arithmetic  6.28 us (2%)
    unnamed x5, waiting for transfers between devices  75.6 us
    all_gather x1, waiting for transfers between devices, per_device(): lax.all_gather((weights - step).astype(jnp.bfloat16), 'fs', axis=0, tiled...  72.9 us
    psum x1, blocking collectives, per_device(): totals = lax.psum(local_sums, ('fs', 'tp'))  39.7 us
    all_gather x1, waiting for transfers between devices, per_device(): whole_factors = lax.all_gather(factors, 'fs', axis=0, tiled=True)  27 us
    unnamed x25, local copies, waits for them, and re-layouts  20.1 us
  transfers between devices with their start and end apart: 4, of which 3 were waited for; matrix products, arithmetic and copies ran while one was open for 10% of the time, Pallas kernels for 0%

commit v1 on v0

--- a/solution.py
+++ b/solution.py
@@ -81,8 +81,22 @@
     rank_here = moments.shape[0]
     cols_here = moments.shape[2]
     factor_wide = factors.astype(jnp.float32)
-    whole_factors = lax.all_gather(factors, "fs", axis=0, tiled=True)
-    reduced = jnp.einsum("td,dkr->tkr", inputs, whole_factors, preferred_element_type=jnp.float32)
+    size, mine, width = (lax.axis_size("fs"), lax.axis_index("fs"), factors.shape[0])
+    right = [(i, (i + 1) % size) for i in range(size)]
+    carried, subtotal = (factors, None)
+    for step_2 in range(size):
+        coming = lax.ppermute(carried, "fs", right) if step_2 < size - 1 else None
+        take_in = jnp.einsum(
+            "td,dkr->tkr",
+            lax.dynamic_slice_in_dim(
+                inputs, (mine - step_2) % size * width, carried.shape[0], axis=1
+            ),
+            carried,
+            preferred_element_type=jnp.float32,
+        )
+        subtotal = take_in if subtotal is None else subtotal + take_in
+        carried = coming
+    reduced = subtotal
     reduced_upper = reduced.astype(jnp.bfloat16)
     reduced_lower = (reduced - reduced_upper.astype(jnp.float32)).astype(jnp.bfloat16)
     upper_part = jnp.einsum(

time: 283 us -> 314 us (1.11)
  waiting for transfers between devices: 176 us -> 200 us
  starting transfers between devices: 0.16 us -> 4.7 us
    ppermute x0 -> x7, waiting for transfers between devices: none -> 52.7 us  [per_device(): coming = lax.ppermute(carried, 'fs', right) if step_2 < size - 1 else None]
    all_gather x1 -> x0, waiting for transfers between devices: 27 us -> none  [per_device(): whole_factors = lax.all_gather(factors, 'fs', axis=0, tiled=True)]
    ppermute x0 -> x7, starting transfers between devices: none -> 4.58 us  [per_device(): coming = lax.ppermute(carried, 'fs', right) if step_2 < size - 1 else None]
    unnamed x5 -> x4, waiting for transfers between devices: 75.6 us -> 74.4 us
    unnamed x25 -> x29, local copies, waits for them, and re-layouts: 20.1 us -> 19.2 us
  transfers between devices with their start and end apart: 4 -> 10, of which waited for: 3 -> 8; matrix products, arithmetic and copies ran while one was open for 10% -> 10% of each run, Pallas kernels for 0% -> 0%
where the time goes in v1:
time: 314 us
  waiting for transfers between devices  200 us (64%)
  blocking collectives  39.7 us (13%)
  local copies, waits for them, and re-layouts  26.9 us (9%)
  matrix products  18.8 us (6%)
  between operations  14.7 us (5%)
  other arithmetic  6.25 us (2%)
  starting transfers between devices  4.7 us (1%)
    unnamed x4, waiting for transfers between devices  74.4 us
    all_gather x1, waiting for transfers between devices, per_device(): lax.all_gather((weights - step).astype(jnp.bfloat16), 'fs', axis=0, tiled...  72.9 us
    ppermute x7, waiting for transfers between devices, per_device(): coming = lax.ppermute(carried, 'fs', right) if step_2 < size - 1 else None  52.7 us
    psum x1, blocking collectives, per_device(): totals = lax.psum(local_sums, ('fs', 'tp'))  39.7 us
    unnamed x29, local copies, waits for them, and re-layouts  19.2 us
  transfers between devices with their start and end apart: 10, of which 8 were waited for; matrix products, arithmetic and copies ran while one was open for 10% of the time, Pallas kernels for 0%

profile of v1, /device:TPU:0, one launch (start us, length us, event | category | flops | bytes accessed | tf_op | source)
XLA Modules:
  0.0 313.8 jit_solution(17152881756715631259)
XLA Ops:
  7.2 1.8 copy.48
  9.1 3.0 collective-permute-start
  12.0 1.2 copy.41
  13.7 1.2 copy.44
  15.0 23.8 %while.12 = (s32[]{:T(128)}, bf16[4,384,128]{1,2,0:T(8,128)(2,1)}, bf16[4,384,128]{2,1,0:T(8,128)(2,1)}, bf16[4,384,2,64]{1,3,2,0:T(8,128)(2,1)S(1)}, bf16[4,384...) while((s32[]{:T(128)}, bf16[4,384,128]{1,2,0:T(8,128)(2,1)}, ...), condition=%wide.region_9.10_spmd, body=%wide.region_0.9_spmd.sunk | while | flops 195525504 | bytes 10978449 | solution.py:73
  15.0 0.6 dynamic_slice.111
  17.1 0.8 subtract_convert_fusion.5
  18.2 1.0 fusion.101
  19.2 0.4 multiply_reduce_fusion.7
  20.3 0.7 constant_dynamic-update-slice_fusion.2
  20.9 0.6 dynamic_slice.111
  22.6 0.3 fusion.95
  23.1 0.8 subtract_convert_fusion.5
  24.2 1.0 fusion.101
  25.2 0.4 multiply_reduce_fusion.7
  26.2 0.7 constant_dynamic-update-slice_fusion.2
  26.9 0.6 dynamic_slice.111
  28.6 0.3 fusion.95
  29.0 0.8 subtract_convert_fusion.5
  30.1 1.0 fusion.101
  31.1 0.4 multiply_reduce_fusion.7
  32.1 0.7 constant_dynamic-update-slice_fusion.2
  32.8 0.6 dynamic_slice.111
  34.9 0.8 subtract_convert_fusion.5
  36.0 1.0 fusion.101
  37.0 0.4 multiply_reduce_fusion.7
  38.1 0.7 constant_dynamic-update-slice_fusion.2
  38.7 1.2 copy.47
  40.3 1.6 collective-permute-start.1
  41.9 1.2 convolution_add_fusion.7
  43.1 7.9 %collective-permute-done.1 = bf16[256,2,256]{2,0,1:T(8,128)(2,1)S(1)} collective-permute-done((bf16[256,2,256]{2,0,1:T(8,128)(2,1)}, bf16[256,2,256]{2,0,1:T(8,128)(2,1)S(1)}, u32[]{:S(2)}, u32[]{:S(2)}) %collective-permute-start.1) | collective-permute-done | bytes 262176 | tf_op jit(solution)/shard_map/ppermute | solution.py:88
  51.3 9.3 %collective-permute-done.2 = bf16[256,2,256]{2,0,1:T(8,128)(2,1)S(1)} collective-permute-done((bf16[256,2,256]{2,0,1:T(8,128)(2,1)S(1)}, bf16[256,2,256]{2,0,1:T(8,128)(2,1)S(1)}, u32[]{:S(2)}, u32[]{:S(2)}) %collective-permute-start.2) | collective-permute-done | bytes 262176 | tf_op jit(solution)/shard_map/ppermute | solution.py:88
  60.9 8.8 %collective-permute-done.3 = bf16[256,2,256]{2,0,1:T(8,128)(2,1)S(1)} collective-permute-done((bf16[256,2,256]{2,0,1:T(8,128)(2,1)S(1)}, bf16[256,2,256]{2,0,1:T(8,128)(2,1)S(1)}, u32[]{:S(2)}, u32[]{:S(2)}) %collective-permute-start.3) | collective-permute-done | bytes 262176 | tf_op jit(solution)/shard_map/ppermute | solution.py:88
  70.0 8.8 %collective-permute-done.4 = bf16[256,2,256]{2,0,1:T(8,128)(2,1)S(1)} collective-permute-done((bf16[256,2,256]{2,0,1:T(8,128)(2,1)S(1)}, bf16[256,2,256]{2,0,1:T(8,128)(2,1)S(1)}, u32[]{:S(2)}, u32[]{:S(2)}) %collective-permute-start.4) | collective-permute-done | bytes 262176 | tf_op jit(solution)/shard_map/ppermute | solution.py:88
  79.1 9.1 %collective-permute-done.5 = bf16[256,2,256]{2,0,1:T(8,128)(2,1)S(1)} collective-permute-done((bf16[256,2,256]{2,0,1:T(8,128)(2,1)S(1)}, bf16[256,2,256]{2,0,1:T(8,128)(2,1)S(1)}, u32[]{:S(2)}, u32[]{:S(2)}) %collective-permute-start.5) | collective-permute-done | bytes 262176 | tf_op jit(solution)/shard_map/ppermute | solution.py:88
  88.4 8.8 %collective-permute-done.6 = bf16[256,2,256]{2,0,1:T(8,128)(2,1)S(1)} collective-permute-done((bf16[256,2,256]{2,0,1:T(8,128)(2,1)S(1)}, bf16[256,2,256]{2,0,1:T(8,128)(2,1)S(1)}, u32[]{:S(2)}, u32[]{:S(2)}) %collective-permute-start.6) | collective-permute-done | bytes 262176 | tf_op jit(solution)/shard_map/ppermute | solution.py:88
  97.5 0.4 fusion.33
  97.9 0.4 fusion.30
  98.4 1.3 copy.50
  99.8 0.6 dynamic-slice
  101.0 74.3 %all-reduce.3.cloned.1.call-done = f32[256,2,512]{2,1,0:T(2,128)} async-done(((f32[256,2,512]{2,1,0:T(2,128)}), f32[256,2,512]{2,1,0:T(2,128)}) %all-reduce.3.cloned.1.call-update) | async-done | bytes 1048592
  175.4 1.8 multiply_reduce_fusion.3
  177.3 1.4 copy.53
  178.7 39.7 %psum.7 = f32[2]{0:T(128)S(1)} all-reduce(f32[2]{0:T(128)S(1)} %get-tuple-element.111), channel_id=1, replica_groups=mesh['fs'=8,'tp'=4] {'fs','tp'}, use_global_device_ids=true, to_apply=%region_12.13 | all-reduce | flops 2 | bytes 16 | tf_op jit(solution)/shard_map/psum | solution.py:112
  218.4 3.5 %subtract_convert_fusion.1 = (bf16[256,2,512]{0,2,1:T(8,128)(2,1)}, f32[256,2,512]{0,2,1:T(8,128)S(1)}) fusion(f32[256,2,512]{0,2,1:T(8,128)} %copy.53, f32[2]{0:T(128)S(1)} %rsqrt_multiply_fusion, bf16[256,2,256]{2,1,0:T(2,128)(2,1)S(1)} %copy-done.1, f32[256,2,512]{2,1,0:T(2,128)} %all-gather.3.cloned.1.call-done), kind=kOutput, calls=%fused_computation.66 | convolution fusion | flops 806092800 | bytes 3932168 | tf_op jit(solution)/shard_map/dkr,rke->dke/dot_general | solution.py:115
  221.9 1.3 copy.54
  223.2 72.9 %all-gather.5.cloned.1.call-done = bf16[2048,2,512]{0,2,1:T(8,128)(2,1)} async-done(((bf16[256,2,512]{0,2,1:T(8,128)(2,1)}), bf16[2048,2,512]{0,2,1:T(8,128)(2,1)}) %all-gather.5.cloned.1.call-update) | async-done | bytes 4194320 | tf_op jit(solution)/shard_map/all_gather | solution.py:122
  296.1 11.1 %copy.55 = bf16[2048,2,512]{2,1,0:T(2,128)(2,1)} copy(bf16[2048,2,512]{0,2,1:T(8,128)(2,1)} %all-gather.5.cloned.1.call-done) | data formatting | bytes 8388608
  (87 shorter events, 8.9 us)
Async XLA Ops:
  7.2 32.8 %copy-start = (bf16[384,2048]{1,0:T(8,128)(2,1)S(1)}, bf16[384,2048]{1,0:T(8,128)(2,1)}, u32[]{:S(2)}) copy-start(bf16[384,2048]{1,0:T(8,128)(2,1)} %param.12) | copy-start | bytes 4718596
  7.2 6.1 %copy-start.4 = (bf16[384,512]{1,0:T(8,128)(2,1)S(1)}, bf16[384,512]{1,0:T(8,128)(2,1)}, u32[]{:S(2)}) copy-start(bf16[384,512]{1,0:T(8,128)(2,1)} %param.14) | copy-start | bytes 1179652
  7.2 6.3 %copy-start.5 = (bf16[384,512]{1,0:T(8,128)(2,1)S(1)}, bf16[384,512]{1,0:T(8,128)(2,1)}, u32[]{:S(2)}) copy-start(bf16[384,512]{1,0:T(8,128)(2,1)} %param.15) | copy-start | bytes 1179652
  7.2 168.2 %all-reduce.3.cloned.1.call-start = ((), (), s32[]{:S(2)}) async-start(), calls=%async_computation.2 | async-start | bytes 2097152
  9.1 31.2 %collective-permute-start = (bf16[256,2,256]{2,0,1:T(8,128)(2,1)}, bf16[256,2,256]{2,0,1:T(8,128)(2,1)}, u32[]{:S(2)}, u32[]{:S(2)}) collective-permute-start(bf16[256,2,256]{2,0,1:T(8,128)(2,1)} %copy.48), channel_id=1, source_target_pairs={{0,4},{4,8},{8,12},{12,16},{16,20},{20,24},{24,28},{28,0},{1,5},{5... | collective-permute-start | bytes 786440 | tf_op jit(solution)/shard_map/ppermute | solution.py:88
  12.0 2.9 copy-start.7
  12.0 2.9 copy-start.8
  15.0 25.0 %copy-start.1 = (bf16[256,2,256]{2,1,0:T(2,128)(2,1)S(1)}, bf16[256,2,256]{2,1,0:T(2,128)(2,1)}, u32[]{:S(2)}) copy-start(bf16[256,2,256]{2,1,0:T(2,128)(2,1)} %param.19) | copy-start | bytes 786436
  40.3 10.7 %collective-permute-start.1 = (bf16[256,2,256]{2,0,1:T(8,128)(2,1)}, bf16[256,2,256]{2,0,1:T(8,128)(2,1)S(1)}, u32[]{:S(2)}, u32[]{:S(2)}) collective-permute-start(bf16[256,2,256]{2,0,1:T(8,128)(2,1)} %collective-permute-done), channel_id=1, source_target_pairs={{0,4},{4,8},{8,12},{12,16},{16,20},{20,24},{24,28},{28,0},{1,5},{5... | collective-permute-start | bytes 786440 | tf_op jit(solution)/shard_map/ppermute | solution.py:88
  51.0 9.6 %collective-permute-start.2 = (bf16[256,2,256]{2,0,1:T(8,128)(2,1)S(1)}, bf16[256,2,256]{2,0,1:T(8,128)(2,1)S(1)}, u32[]{:S(2)}, u32[]{:S(2)}) collective-permute-start(bf16[256,2,256]{2,0,1:T(8,128)(2,1)S(1)} %collective-permute-done.1), channel_id=1, source_target_pairs={{0,4},{4,8},{8,12},{12,16},{16,20},{20,24},{24,28},{28,0},{1,5},{5... | collective-permute-start | bytes 786440 | tf_op jit(solution)/shard_map/ppermute | solution.py:88
  60.6 9.1 %collective-permute-start.3 = (bf16[256,2,256]{2,0,1:T(8,128)(2,1)S(1)}, bf16[256,2,256]{2,0,1:T(8,128)(2,1)S(1)}, u32[]{:S(2)}, u32[]{:S(2)}) collective-permute-start(bf16[256,2,256]{2,0,1:T(8,128)(2,1)S(1)} %collective-permute-done.2), channel_id=1, source_target_pairs={{0,4},{4,8},{8,12},{12,16},{16,20},{20,24},{24,28},{28,0},{1,5},{5... | collective-permute-start | bytes 786440 | tf_op jit(solution)/shard_map/ppermute | solution.py:88
  69.7 9.1 %collective-permute-start.4 = (bf16[256,2,256]{2,0,1:T(8,128)(2,1)S(1)}, bf16[256,2,256]{2,0,1:T(8,128)(2,1)S(1)}, u32[]{:S(2)}, u32[]{:S(2)}) collective-permute-start(bf16[256,2,256]{2,0,1:T(8,128)(2,1)S(1)} %collective-permute-done.3), channel_id=1, source_target_pairs={{0,4},{4,8},{8,12},{12,16},{16,20},{20,24},{24,28},{28,0},{1,5},{5... | collective-permute-start | bytes 786440 | tf_op jit(solution)/shard_map/ppermute | solution.py:88
  78.8 9.4 %collective-permute-start.5 = (bf16[256,2,256]{2,0,1:T(8,128)(2,1)S(1)}, bf16[256,2,256]{2,0,1:T(8,128)(2,1)S(1)}, u32[]{:S(2)}, u32[]{:S(2)}) collective-permute-start(bf16[256,2,256]{2,0,1:T(8,128)(2,1)S(1)} %collective-permute-done.4), channel_id=1, source_target_pairs={{0,4},{4,8},{8,12},{12,16},{16,20},{20,24},{24,28},{28,0},{1,5},{5... | collective-permute-start | bytes 786440 | tf_op jit(solution)/shard_map/ppermute | solution.py:88
  79.0 18.4 %copy-start.2 = (bf16[4,384,128]{1,2,0:T(8,128)(2,1)S(1)}, bf16[4,384,128]{1,2,0:T(8,128)(2,1)}, u32[]{:S(2)}) copy-start(bf16[4,384,128]{1,2,0:T(8,128)(2,1)} %get-tuple-element.51) | copy-start | bytes 1179652
  88.2 9.1 %collective-permute-start.6 = (bf16[256,2,256]{2,0,1:T(8,128)(2,1)S(1)}, bf16[256,2,256]{2,0,1:T(8,128)(2,1)S(1)}, u32[]{:S(2)}, u32[]{:S(2)}) collective-permute-start(bf16[256,2,256]{2,0,1:T(8,128)(2,1)S(1)} %collective-permute-done.5), channel_id=1, source_target_pairs={{0,4},{4,8},{8,12},{12,16},{16,20},{20,24},{24,28},{28,0},{1,5},{5... | collective-permute-start | bytes 786440 | tf_op jit(solution)/shard_map/ppermute | solution.py:88
  98.4 1.4 copy-start.9
  98.4 77.0 %copy-start.6 = (f32[32,2,512]{2,1,0:T(2,128)S(1)}, f32[32,2,512]{2,1,0:T(2,128)}, u32[]{:S(2)}) copy-start(f32[32,2,512]{2,1,0:T(2,128)} %param.20) | copy-start | bytes 393220
  99.7 77.5 %copy-start.3 = (f32[256,2,512]{2,1,0:T(2,128)S(1)}, f32[256,2,512]{2,1,0:T(2,128)}, u32[]{:S(2)}) copy-start(f32[256,2,512]{2,1,0:T(2,128)} %param.21) | copy-start | bytes 3145732
  99.7 118.7 %all-gather.3.cloned.1.call-start = ((), (), s32[]{:S(2)}) async-start(), calls=%async_computation | async-start | bytes 1179648 | tf_op jit(solution)/shard_map/all_gather | solution.py:118
  177.2 118.9 %all-gather.5.cloned.1.call-start = ((), (), s32[]{:S(2)}) async-start(), calls=%async_computation.1 | async-start | bytes 4718592 | tf_op jit(solution)/shard_map/all_gather | solution.py:122
Sparse Core Ops, SparseCore 0:
  99.9 75.4 all-reduce.2
  178.1 40.0 all-gather.2
  222.0 74.0 all-gather.4
